TPU v7x, 32 devices: a whole 2x2x4 slice. The times are simulated.
32 devices in a mesh: kv: 8 (over z, y), tp: 4 (over x, core).
Axes of the slice: x: 2, y: 2, z: 4, core: 2. Of those that a mesh axis runs over, the one named last changes fastest.
Arguments:
- x_piece: bfloat16 [128, 2048], P('kv'), may hold values from -6 to 6
- x_decode: bfloat16 [8, 2048], P('kv'), may hold values from -6 to 6
- norm_gain: float32 [2048], replicated, may hold values from 0.1 to 1.9
- w_query: bfloat16 [2048, 1024], P(None, 'tp'), may hold values from -0.1875 to 0.1875
- w_key: bfloat16 [2048, 1024], P(None, 'tp'), may hold values from -0.1875 to 0.1875
- w_value: bfloat16 [2048, 1024], P(None, 'tp'), may hold values from -0.125 to 0.125
- w_out: bfloat16 [1024, 2048], P(None, 'tp'), may hold values from -0.1875 to 0.1875
- head_gain: float32 [128], replicated, may hold values from 0.1 to 1.9
- lambdas: float32 [8], P('tp'), may hold values from 0.3 to 0.8
- piece_keys: bfloat16 [4096, 8, 128], P('kv', 'tp'), may hold values from -300 to 300
- piece_values: bfloat16 [4096, 8, 128], P('kv', 'tp'), may hold values from -6 to 6
- cache_keys: bfloat16 [8, 2048, 8, 128], P('kv', None, 'tp'), may hold values from -300 to 300
- cache_values: bfloat16 [8, 2048, 8, 128], P('kv', None, 'tp'), may hold values from -6 to 6
- cache_lengths: int32 [8], P('kv'), may hold values from 1 to 2048, as said below
Outputs:
- piece_out: bfloat16 [128, 2048], P('kv', 'tp')
- decode_out: bfloat16 [8, 2048], P('kv', 'tp')
Inputs may be any that keep to these rules, and one draw needn't show every extreme that they name: `cache_lengths`: some sequence has exactly 2048 filled slots.
All inputs are finite; a program needn't handle non-finite values.
Results may differ from a plain program's by a relative error of at most 0.013.
The roundings to bfloat16 on the way count: a program that leaves them out, or rounds other values in their place, can miss the bound.
Values may be sent and summed in bfloat16 or wider, within the bound.
A program may use at most 64 MiB of HBM per device.

v0:
```python
import math
import jax
import jax.numpy as jnp
from jax import lax
from jax.sharding import PartitionSpec as P

EPS = 1e-06


def shards(
    x_piece,
    x_decode,
    norm_gain,
    w_query,
    w_key,
    w_value,
    w_out,
    head_gain,
    lambdas,
    piece_keys,
    piece_values,
    cache_keys,
    cache_values,
    cache_lengths,
):
    piece_rows = x_piece.shape[0]
    local_heads = lambdas.shape[0]
    pair_width = piece_keys.shape[2]
    half_width = pair_width // 2
    value_width = piece_values.shape[2]
    score_scale = 1.0 / math.sqrt(half_width)
    cached = piece_keys.shape[0]
    all_rows = jnp.concatenate([x_piece, x_decode], axis=0)
    row_count = all_rows.shape[0]
    rows32 = all_rows.astype(jnp.float32)
    normed = (
        rows32 * lax.rsqrt(jnp.mean(rows32 * rows32, axis=-1, keepdims=True) + EPS) * norm_gain
    ).astype(jnp.bfloat16)
    queries = (
        jnp.dot(normed, w_query, preferred_element_type=jnp.float32)
        .astype(jnp.bfloat16)
        .reshape(row_count, local_heads, pair_width)
    )
    new_keys = (
        jnp.dot(normed, w_key, preferred_element_type=jnp.float32)
        .astype(jnp.bfloat16)
        .reshape(row_count, local_heads, pair_width)
    )
    new_values = (
        jnp.dot(normed, w_value, preferred_element_type=jnp.float32)
        .astype(jnp.bfloat16)
        .reshape(row_count, local_heads, value_width)
    )
    keys_all = jnp.concatenate([piece_keys, new_keys[:piece_rows]], axis=0)
    values_all = jnp.concatenate([piece_values, new_values[:piece_rows]], axis=0)
    offset = lax.axis_index("kv") * piece_rows
    kv_count = lax.axis_size("kv")
    total_rows = piece_rows * kv_count
    key_index = jnp.arange(cached + piece_rows, dtype=jnp.int32)

    def block_terms(query_block, block_start):
        block_rows = query_block.shape[0]
        query_pos = block_start + jnp.arange(block_rows, dtype=jnp.int32)
        allowed = (key_index[None, :] < cached) | (
            key_index[None, :] - cached + offset <= query_pos[:, None]
        )
        results = []
        for which_map in range(2):
            lower = which_map * half_width
            scores = (
                jnp.einsum(
                    "qhd,khd->hqk",
                    query_block[:, :, lower : lower + half_width],
                    keys_all[:, :, lower : lower + half_width],
                    preferred_element_type=jnp.float32,
                )
                * score_scale
            )
            scores = jnp.where(allowed[None], scores, -jnp.inf)
            row_max = jnp.max(scores, axis=-1)
            weights = jnp.exp(scores - row_max[..., None])
            totals = jnp.sum(weights, axis=-1)
            mixed = jnp.einsum(
                "hqk,khd->qhd",
                weights.astype(jnp.bfloat16),
                values_all,
                preferred_element_type=jnp.float32,
            )
            results += [row_max, totals, mixed.reshape(block_rows, local_heads * value_width)]
        return tuple(results)

    stat_zeros = jnp.zeros((local_heads, total_rows), jnp.float32)
    value_zeros = jnp.zeros((total_rows, local_heads * value_width), jnp.float32)
    initial = (stat_zeros, stat_zeros, value_zeros, stat_zeros, stat_zeros, value_zeros)
    piece = lax.all_gather(queries[:piece_rows], "kv", axis=0, tiled=True)
    start = jnp.int32(0)
    block_rows = piece.shape[0]
    if block_rows > 512 and block_rows % 512 == 0:
        nblocks = block_rows // 512
        blocks = piece.reshape(nblocks, 512, local_heads, pair_width)
        starts = start + 512 * jnp.arange(nblocks, dtype=jnp.int32)
        mapped = lax.map(lambda inputs: block_terms(inputs[0], inputs[1]), (blocks, starts))
        results = []
        for index, entry in enumerate(mapped):
            if index % 3 == 2:
                results.append(entry.reshape(block_rows, local_heads * value_width))
            else:
                results.append(entry.transpose(1, 0, 2).reshape(local_heads, block_rows))
        results = tuple(results)
    else:
        results = block_terms(piece, start)
    updated = []
    for index in range(6):
        along = 0 if index % 3 == 2 else 1
        updated.append(
            lax.dynamic_update_slice_in_dim(initial[index], results[index], start, along)
        )
    partials = tuple(updated)
    moved_values = (
        lax.all_to_all(
            partials[2].astype(jnp.bfloat16), "kv", split_axis=0, concat_axis=0, tiled=True
        ).astype(jnp.float32),
        lax.all_to_all(
            partials[5].astype(jnp.bfloat16), "kv", split_axis=0, concat_axis=0, tiled=True
        ).astype(jnp.float32),
    )
    moved_stats = (
        lax.all_to_all(partials[0], "kv", split_axis=1, concat_axis=1, tiled=True),
        lax.all_to_all(partials[1], "kv", split_axis=1, concat_axis=1, tiled=True),
        lax.all_to_all(partials[3], "kv", split_axis=1, concat_axis=1, tiled=True),
        lax.all_to_all(partials[4], "kv", split_axis=1, concat_axis=1, tiled=True),
    )
    own = []
    for which_map in range(2):
        maxima = moved_stats[2 * which_map].reshape(local_heads, kv_count, piece_rows)
        sums = moved_stats[2 * which_map + 1].reshape(local_heads, kv_count, piece_rows)
        weighted = moved_values[which_map].reshape(kv_count, piece_rows, local_heads * value_width)
        new_max = jnp.max(maxima, axis=1)
        factor = jnp.exp(maxima - new_max[:, None, :])
        value_factor = jnp.repeat(factor.transpose(1, 2, 0), value_width, axis=2)
        own += [new_max, jnp.sum(factor * sums, axis=1), jnp.sum(value_factor * weighted, axis=0)]
    lambda_wide = jnp.repeat(lambdas, value_width)[None, :]
    piece_mixed = own[2] / jnp.repeat(own[1].T, value_width, axis=1) - lambda_wide * own[
        5
    ] / jnp.repeat(own[4].T, value_width, axis=1)
    dec_query = queries[piece_rows:]
    own_keys = new_keys[piece_rows:]
    own_values = new_values[piece_rows:].astype(jnp.float32)
    slot_index = jnp.arange(cache_keys.shape[1], dtype=jnp.int32)
    slot_allowed = slot_index[None, None, :] < cache_lengths[:, None, None]
    dec_results = []
    for which_map in range(2):
        lower = which_map * half_width
        scores = (
            jnp.einsum(
                "bhd,bkhd->bhk",
                dec_query[:, :, lower : lower + half_width],
                cache_keys[:, :, :, lower : lower + half_width],
                preferred_element_type=jnp.float32,
            )
            * score_scale
        )
        scores = jnp.where(slot_allowed, scores, -jnp.inf)
        own_score = (
            jnp.einsum(
                "bhd,bhd->bh",
                dec_query[:, :, lower : lower + half_width],
                own_keys[:, :, lower : lower + half_width],
                preferred_element_type=jnp.float32,
            )
            * score_scale
        )
        row_max = jnp.maximum(jnp.max(scores, axis=-1), own_score)
        weights = jnp.exp(scores - row_max[..., None])
        own_weight = jnp.exp(own_score - row_max)
        totals = jnp.sum(weights, axis=-1) + own_weight
        mixed = jnp.einsum(
            "bhk,bkhd->bhd",
            weights.astype(jnp.bfloat16),
            cache_values,
            preferred_element_type=jnp.float32,
        )
        mixed = mixed + own_weight.astype(jnp.bfloat16).astype(jnp.float32)[..., None] * own_values
        dec_results.append(mixed / totals[..., None])
    dec_mixed = (dec_results[0] - lambdas[None, :, None] * dec_results[1]).reshape(
        -1, local_heads * value_width
    )
    attended = jnp.concatenate([piece_mixed, dec_mixed], axis=0).reshape(
        row_count, local_heads, value_width
    )
    head_out = (
        attended
        * lax.rsqrt(jnp.mean(attended * attended, axis=-1, keepdims=True) + EPS)
        * head_gain
    ).astype(jnp.bfloat16)
    head_out = head_out.reshape(row_count, local_heads * value_width)
    output = jnp.dot(
        lax.all_gather(head_out, "tp", axis=1, tiled=True),
        w_out,
        preferred_element_type=jnp.float32,
    )
    output = output.astype(jnp.bfloat16)
    return (output[:piece_rows], output[piece_rows:])


def solution(mesh):
    placed = (
        P("kv", None),
        P("kv", None),
        P(),
        P(None, "tp"),
        P(None, "tp"),
        P(None, "tp"),
        P(None, "tp"),
        P(),
        P("tp"),
        P("kv", "tp", None),
        P("kv", "tp", None),
        P("kv", None, "tp", None),
        P("kv", None, "tp", None),
        P("kv"),
    )
    return jax.shard_map(
        shards,
        mesh=mesh,
        in_specs=placed,
        out_specs=(P("kv", "tp"), P("kv", "tp")),
        check_vma=False,
    )
```

profile of v0, /device:TPU:0, one launch (start us, length us, event | category | flops | bytes accessed | tf_op | source)
XLA Modules:
  0.0 112.1 jit_solution(12364098062893879880)
XLA Ops:
  0.7 1.1 %fusion.21 = f32[17]{0:T(128)S(1)} fusion(bf16[1,2048]{1,0:T(2,128)(2,1)} %param.15, bf16[16,2048]{1,0:T(8,128)(2,1)} %param.14), kind=kLoop, calls=%fused_computation.37 | loop fusion | flops 208879 | bytes 69700 | tf_op jit(solution)/shard_map/reduce_sum | solution.py:37
  1.9 1.6 %convolution_convert_fusion.5 = bf16[17,256]{1,0:T(8,128)(2,1)S(1)} fusion(bf16[2048,256]{1,0:T(8,128)(2,1)} %param.17, f32[2048]{0:T(1024)} %param.16, f32[17]{0:T(128)S(1)} %add_rsqrt_fusion.1, bf16[1,2048]{1,0:T(2,128)(2,1)} %param.15, bf16[16,2048]{1,0:T(8,128)(2,1)S(1)} %copy-done.2), kind=kOutput, calls=%fused_computation.11 | convolution fusion | flops 18073856 | bytes 1135172 | tf_op jit(solution)/shard_map/dot_general | solution.py:40
  3.8 32.5 %all_gather.6 = bf16[128,2,128]{2,1,0:T(2,128)(2,1)S(1)} all-gather(bf16[16,2,128]{2,1,0:T(2,128)(2,1)S(1)} %slice.73), channel_id=1, replica_groups=mesh['kv'=8,'tp'=4] {'kv'}, dimensions={0}, use_global_device_ids=true | all-gather | bytes 73728 | tf_op jit(solution)/shard_map/all_gather | solution.py:95
  37.4 0.6 copy.77
  38.0 5.5 %all-to-all-start.5 = ((f32[2,8,16]{2,0,1:T(2,128)}), f32[2,8,16]{2,0,1:T(2,128)S(1)}, u32[]{:S(2)}, u32[]{:S(2)}) async-start(f32[2,8,16]{2,0,1:T(2,128)} %copy.77), calls=%async_computation.5 | async-start | bytes 16384 | tf_op jit(solution)/shard_map/all_to_all | solution.py:131
  43.7 1.9 %slice_bitcast_fusion = (bf16[2048,2,64]{2,1,0:T(2,128)(2,1)S(1)}, bf16[2048,2,64]{2,1,0:T(2,128)(2,1)S(1)}) fusion(bf16[1,2048,2,128]{3,2,1,0:T(2,128)(2,1)S(1)} %copy-done.1), kind=kLoop, calls=%fused_computation.16 | loop fusion | bytes 2097152 | tf_op jit(solution)/shard_map/reshape.43
  48.1 0.7 copy-done.4
  49.1 0.6 copy-done.7
  50.8 0.6 copy-done.10
  52.2 6.1 %all-to-all-start.3 = ((f32[2,8,16]{2,0,1:T(2,128)}), f32[2,8,16]{2,0,1:T(2,128)S(1)}, u32[]{:S(2)}, u32[]{:S(2)}) async-start(f32[2,8,16]{2,0,1:T(2,128)} %copy.74), calls=%async_computation.3 | async-start | bytes 16384 | tf_op jit(solution)/shard_map/all_to_all | solution.py:130
  59.1 5.8 %all-to-all-done.3 = f32[2,8,16]{2,0,1:T(2,128)S(1)} async-done(((f32[2,8,16]{2,0,1:T(2,128)}), f32[2,8,16]{2,0,1:T(2,128)S(1)}, u32[]{:S(2)}, u32[]{:S(2)}) %all-to-all-start.3) | async-done | bytes 1056 | tf_op jit(solution)/shard_map/all_to_all | solution.py:130
  64.9 3.3 %all-to-all-start = ((f32[2,8,16]{2,0,1:T(2,128)}), f32[2,8,16]{2,0,1:T(2,128)S(1)}, u32[]{:S(2)}, u32[]{:S(2)}) async-start(f32[2,8,16]{2,0,1:T(2,128)} %copy.65), calls=%async_computation | async-start | bytes 16384 | tf_op jit(solution)/shard_map/all_to_all | solution.py:128
  68.4 0.7 convert_element_type.100
  69.2 0.6 copy.70
  69.9 0.7 convert_element_type.95
  70.6 4.1 %all-to-all-done = f32[2,8,16]{2,0,1:T(2,128)S(1)} async-done(((f32[2,8,16]{2,0,1:T(2,128)}), f32[2,8,16]{2,0,1:T(2,128)S(1)}, u32[]{:S(2)}, u32[]{:S(2)}) %all-to-all-start) | async-done | bytes 1056 | tf_op jit(solution)/shard_map/all_to_all | solution.py:128
  74.7 3.3 %all-to-all-start.2 = ((f32[2,8,16]{2,0,1:T(2,128)}), f32[2,8,16]{2,0,1:T(2,128)S(1)}, u32[]{:S(2)}, u32[]{:S(2)}) async-start(f32[2,8,16]{2,0,1:T(2,128)} %copy.70), calls=%async_computation.2 | async-start | bytes 16384 | tf_op jit(solution)/shard_map/all_to_all | solution.py:129
  78.5 6.0 %all-to-all-done.2 = f32[2,8,16]{2,0,1:T(2,128)S(1)} async-done(((f32[2,8,16]{2,0,1:T(2,128)}), f32[2,8,16]{2,0,1:T(2,128)S(1)}, u32[]{:S(2)}, u32[]{:S(2)}) %all-to-all-start.2) | async-done | bytes 1056 | tf_op jit(solution)/shard_map/all_to_all | solution.py:129
  84.5 3.3 %all-to-all-start.4 = ((bf16[8,16,256]{2,1,0:T(8,128)(2,1)}), bf16[8,16,256]{2,1,0:T(8,128)(2,1)S(1)}, u32[]{:S(2)}, u32[]{:S(2)}) async-start(bf16[8,16,256]{2,1,0:T(8,128)(2,1)} %convert_element_type.100), calls=%async_computation.4 | async-start | bytes 131072 | tf_op jit(solution)/shard_map/all_to_all | solution.py:123
  88.5 6.2 %all-to-all-done.4 = bf16[8,16,256]{2,1,0:T(8,128)(2,1)S(1)} async-done(((bf16[8,16,256]{2,1,0:T(8,128)(2,1)}), bf16[8,16,256]{2,1,0:T(8,128)(2,1)S(1)}, u32[]{:S(2)}, u32[]{:S(2)}) %all-to-all-start.4) | async-done | bytes 65568 | tf_op jit(solution)/shard_map/all_to_all | solution.py:123
  94.7 3.3 %all-to-all-start.1 = ((bf16[8,16,256]{2,1,0:T(8,128)(2,1)}), bf16[8,16,256]{2,1,0:T(8,128)(2,1)S(1)}, u32[]{:S(2)}, u32[]{:S(2)}) async-start(bf16[8,16,256]{2,1,0:T(8,128)(2,1)} %convert_element_type.95), calls=%async_computation.1 | async-start | bytes 131072 | tf_op jit(solution)/shard_map/all_to_all | solution.py:120
  98.1 6.8 %all-to-all-done.1 = bf16[8,16,256]{2,1,0:T(8,128)(2,1)S(1)} async-done(((bf16[8,16,256]{2,1,0:T(8,128)(2,1)}), bf16[8,16,256]{2,1,0:T(8,128)(2,1)S(1)}, u32[]{:S(2)}, u32[]{:S(2)}) %all-to-all-start.1) | async-done | bytes 65568 | tf_op jit(solution)/shard_map/all_to_all | solution.py:120
  105.5 5.2 %all_gather.7 = bf16[17,1024]{1,0:T(8,128)(2,1)S(1)} all-gather(bf16[17,256]{1,0:T(8,128)(2,1)S(1)} %fusion.30), channel_id=1, replica_groups=mesh['kv'=8,'tp'=4] {'tp'}, dimensions={1}, use_global_device_ids=true | all-gather | bytes 43520 | tf_op jit(solution)/shard_map/all_gather | solution.py:198
  110.9 0.6 slice.105
  (95 shorter events, 9.2 us)
Async XLA Ops:
  0.6 47.0 %copy-start = (bf16[1,2048,2,128]{3,2,1,0:T(2,128)(2,1)S(1)}, bf16[1,2048,2,128]{3,2,1,0:T(2,128)(2,1)}, u32[]{:S(2)}) copy-start(bf16[1,2048,2,128]{3,2,1,0:T(2,128)(2,1)} %param.26) | copy-start | bytes 3145732
  0.6 1.2 %copy-start.2 = (bf16[16,2048]{1,0:T(8,128)(2,1)S(1)}, bf16[16,2048]{1,0:T(8,128)(2,1)}, u32[]{:S(2)}) copy-start(bf16[16,2048]{1,0:T(8,128)(2,1)} %param.14) | copy-start | bytes 196612
  0.7 2.8 %copy-start.3 = (bf16[2048,256]{1,0:T(8,128)(2,1)S(1)}, bf16[2048,256]{1,0:T(8,128)(2,1)}, u32[]{:S(2)}) copy-start(bf16[2048,256]{1,0:T(8,128)(2,1)} %param.18) | copy-start | bytes 3145732
  1.8 1.6 %copy-start.8 = (bf16[1,2048]{1,0:T(2,128)(2,1)S(1)}, bf16[1,2048]{1,0:T(2,128)(2,1)}, u32[]{:S(2)}) copy-start(bf16[1,2048]{1,0:T(2,128)(2,1)} %param.15) | copy-start | bytes 12292
  1.8 1.6 %copy-start.9 = (f32[2048]{0:T(1024)S(1)}, f32[2048]{0:T(1024)}, u32[]{:S(2)}) copy-start(f32[2048]{0:T(1024)} %param.16) | copy-start | bytes 24580
  3.8 32.8 %copy-start.6 = (bf16[512,2,128]{2,1,0:T(2,128)(2,1)S(1)}, bf16[512,2,128]{2,1,0:T(2,128)(2,1)}, u32[]{:S(2)}) copy-start(bf16[512,2,128]{2,1,0:T(2,128)(2,1)} %param.23) | copy-start | bytes 786436
  36.5 7.1 %copy-start.1 = (bf16[1,2048,2,128]{3,2,1,0:T(2,128)(2,1)S(1)}, bf16[1,2048,2,128]{3,2,1,0:T(2,128)(2,1)}, u32[]{:S(2)}) copy-start(bf16[1,2048,2,128]{3,2,1,0:T(2,128)(2,1)} %param.25) | copy-start | bytes 3145732
  38.0 14.2 %all-to-all-start.5 = ((f32[2,8,16]{2,0,1:T(2,128)}), f32[2,8,16]{2,0,1:T(2,128)S(1)}, u32[]{:S(2)}, u32[]{:S(2)}) async-start(f32[2,8,16]{2,0,1:T(2,128)} %copy.77), calls=%async_computation.5 | async-start | bytes 16384 | tf_op jit(solution)/shard_map/all_to_all | solution.py:131
  47.6 1.2 %copy-start.4 = (bf16[2048,256]{1,0:T(8,128)(2,1)S(1)}, bf16[2048,256]{1,0:T(8,128)(2,1)}, u32[]{:S(2)}) copy-start(bf16[2048,256]{1,0:T(8,128)(2,1)} %param.19) | copy-start | bytes 3145732
  48.8 0.9 copy-start.7
  50.8 0.7 copy-start.10
  52.2 6.1 %copy-start.11 = (f32[128]{0:T(128)S(1)}, f32[128]{0:T(128)}, u32[]{:S(2)}) copy-start(f32[128]{0:T(128)} %param.21) | copy-start | bytes 1540
  52.2 12.7 %all-to-all-start.3 = ((f32[2,8,16]{2,0,1:T(2,128)}), f32[2,8,16]{2,0,1:T(2,128)S(1)}, u32[]{:S(2)}, u32[]{:S(2)}) async-start(f32[2,8,16]{2,0,1:T(2,128)} %copy.74), calls=%async_computation.3 | async-start | bytes 16384 | tf_op jit(solution)/shard_map/all_to_all | solution.py:130
  64.9 9.8 %all-to-all-start = ((f32[2,8,16]{2,0,1:T(2,128)}), f32[2,8,16]{2,0,1:T(2,128)S(1)}, u32[]{:S(2)}, u32[]{:S(2)}) async-start(f32[2,8,16]{2,0,1:T(2,128)} %copy.65), calls=%async_computation | async-start | bytes 16384 | tf_op jit(solution)/shard_map/all_to_all | solution.py:128
  74.7 9.8 %all-to-all-start.2 = ((f32[2,8,16]{2,0,1:T(2,128)}), f32[2,8,16]{2,0,1:T(2,128)S(1)}, u32[]{:S(2)}, u32[]{:S(2)}) async-start(f32[2,8,16]{2,0,1:T(2,128)} %copy.70), calls=%async_computation.2 | async-start | bytes 16384 | tf_op jit(solution)/shard_map/all_to_all | solution.py:129
  78.4 32.3 %copy-start.5 = (bf16[1024,512]{1,0:T(8,128)(2,1)S(1)}, bf16[1024,512]{1,0:T(8,128)(2,1)}, u32[]{:S(2)}) copy-start(bf16[1024,512]{1,0:T(8,128)(2,1)} %param.20) | copy-start | bytes 3145732
  84.5 10.2 %all-to-all-start.4 = ((bf16[8,16,256]{2,1,0:T(8,128)(2,1)}), bf16[8,16,256]{2,1,0:T(8,128)(2,1)S(1)}, u32[]{:S(2)}, u32[]{:S(2)}) async-start(bf16[8,16,256]{2,1,0:T(8,128)(2,1)} %convert_element_type.100), calls=%async_computation.4 | async-start | bytes 131072 | tf_op jit(solution)/shard_map/all_to_all | solution.py:123
  94.7 10.2 %all-to-all-start.1 = ((bf16[8,16,256]{2,1,0:T(8,128)(2,1)}), bf16[8,16,256]{2,1,0:T(8,128)(2,1)S(1)}, u32[]{:S(2)}, u32[]{:S(2)}) async-start(bf16[8,16,256]{2,1,0:T(8,128)(2,1)} %convert_element_type.95), calls=%async_computation.1 | async-start | bytes 131072 | tf_op jit(solution)/shard_map/all_to_all | solution.py:120
where the time goes:
time: 113 us; the launch traced here: 112 us
  blocking collectives  37.7 us (33%)
  waiting for transfers between devices  28.8 us (25%)
  starting transfers between devices  25 us (22%)
  local copies, waits for them, and re-layouts  11.4 us (10%)
  matrix products  4.9 us (4%)
  other arithmetic  2.63 us (2%)
  between operations  1.7 us (2%)
    all_gather x1, blocking collectives, shards(): piece = lax.all_gather(queries[:piece_rows], 'kv', axis=0, tiled=True)  32.5 us
    all_to_all x1, waiting for transfers between devices, shards(): lax.all_to_all(partials[2].astype(jnp.bfloat16), 'kv', split_axis=0, conc...  6.8 us
    all_to_all x1, waiting for transfers between devices, shards(): lax.all_to_all(partials[5].astype(jnp.bfloat16), 'kv', split_axis=0, conc...  6.2 us
    all_to_all x1, starting transfers between devices, shards(): lax.all_to_all(partials[3], 'kv', split_axis=1, concat_axis=1, tiled=True)  6.13 us
    all_to_all x1, waiting for transfers between devices, shards(): lax.all_to_all(partials[1], 'kv', split_axis=1, concat_axis=1, tiled=True)  5.96 us
    all_to_all x1, waiting for transfers between devices, shards(): lax.all_to_all(partials[3], 'kv', split_axis=1, concat_axis=1, tiled=True)  5.82 us
    all_to_all x1, starting transfers between devices, shards(): lax.all_to_all(partials[4], 'kv', split_axis=1, concat_axis=1, tiled=True)  5.49 us
    all_gather x1, blocking collectives, shards(): lax.all_gather(head_out, 'tp', axis=1, tiled=True)  5.22 us
  transfers between devices with their start and end apart: 6, of which 5 were waited for; matrix products, arithmetic and copies ran while one was open for 9% of the time, Pallas kernels for 0%

commit v1 on v0

--- a/solution.py
+++ b/solution.py
@@ -126,7 +126,12 @@
     )
     moved_stats = (
         lax.all_to_all(partials[0], "kv", split_axis=1, concat_axis=1, tiled=True),
-        lax.all_to_all(partials[1], "kv", split_axis=1, concat_axis=1, tiled=True),
+        jnp.concatenate(
+            lax.all_to_all(
+                jnp.stack(jnp.split(partials[1], lax.axis_size("kv"), axis=1)), "kv", 0, 0
+            ),
+            axis=1,
+        ),
         lax.all_to_all(partials[3], "kv", split_axis=1, concat_axis=1, tiled=True),
         lax.all_to_all(partials[4], "kv", split_axis=1, concat_axis=1, tiled=True),
     )

time: 113 us -> 117 us (1.035)
  local copies, waits for them, and re-layouts: 11.4 us -> 15.7 us
    all_to_all x1, waiting for transfers between devices: 5.96 us -> 0.01 us  [shards(): lax.all_to_all(jnp.stack(jnp.split(partials[1], lax.axis_size('kv'), axis...]
    all_to_all x1, waiting for transfers between devices: 0.01 us -> 5.96 us  [shards(): lax.all_to_all(partials[4], 'kv', split_axis=1, concat_axis=1, tiled=True)]
    unnamed x28 -> x35, local copies, waits for them, and re-layouts: 2.28 us -> 6.64 us
    all_to_all x1, starting transfers between devices: 6.13 us -> 3.31 us  [shards(): lax.all_to_all(partials[3], 'kv', split_axis=1, concat_axis=1, tiled=True)]
    all_to_all x1, starting transfers between devices: 3.31 us -> 6.13 us  [shards(): lax.all_to_all(partials[0], 'kv', split_axis=1, concat_axis=1, tiled=True)]
    all_to_all x1, starting transfers between devices: 3.33 us -> 5.49 us  [shards(): lax.all_to_all(jnp.stack(jnp.split(partials[1], lax.axis_size('kv'), axis...]
    all_to_all x1, starting transfers between devices: 5.49 us -> 3.33 us  [shards(): lax.all_to_all(partials[4], 'kv', split_axis=1, concat_axis=1, tiled=True)]
    all_to_all x1, waiting for transfers between devices: 4.06 us -> 5.82 us  [shards(): lax.all_to_all(partials[0], 'kv', split_axis=1, concat_axis=1, tiled=True)]
where the time goes in v1:
time: 117 us; the launch traced here: 116 us
  blocking collectives  37.7 us (32%)
  waiting for transfers between devices  28.8 us (25%)
  starting transfers between devices  25 us (21%)
  local copies, waits for them, and re-layouts  15.7 us (13%)
  matrix products  4.9 us (4%)
  other arithmetic  2.63 us (2%)
  between operations  1.72 us (1%)
    all_gather x1, blocking collectives, shards(): piece = lax.all_gather(queries[:piece_rows], 'kv', axis=0, tiled=True)  32.5 us
    all_to_all x1, waiting for transfers between devices, shards(): lax.all_to_all(partials[5].astype(jnp.bfloat16), 'kv', split_axis=0, conc...  6.8 us
    unnamed x35, local copies, waits for them, and re-layouts  6.64 us
    all_to_all x1, waiting for transfers between devices, shards(): lax.all_to_all(partials[2].astype(jnp.bfloat16), 'kv', split_axis=0, conc...  6.2 us
    all_to_all x1, starting transfers between devices, shards(): lax.all_to_all(partials[0], 'kv', split_axis=1, concat_axis=1, tiled=True)  6.13 us
    all_to_all x1, waiting for transfers between devices, shards(): lax.all_to_all(partials[4], 'kv', split_axis=1, concat_axis=1, tiled=True)  5.96 us
    all_to_all x1, waiting for transfers between devices, shards(): lax.all_to_all(partials[0], 'kv', split_axis=1, concat_axis=1, tiled=True)  5.82 us
    all_to_all x1, starting transfers between devices, shards(): lax.all_to_all(jnp.stack(jnp.split(partials[1], lax.axis_size('kv'), axis...  5.49 us
  transfers between devices with their start and end apart: 6, of which 5 were waited for; matrix products, arithmetic and copies ran while one was open for 9% of the time, Pallas kernels for 0%

profile of v1, /device:TPU:0, one launch (start us, length us, event | category | flops | bytes accessed | tf_op | source)
XLA Modules:
  0.0 116.5 jit_solution(283161740637802570)
XLA Ops:
  0.7 1.1 fusion.21
  1.9 1.6 %convolution_convert_fusion.4 = bf16[17,256]{1,0:T(8,128)(2,1)S(1)} fusion(bf16[2048,256]{1,0:T(8,128)(2,1)} %param.18, f32[2048]{0:T(1024)} %param.16, f32[17]{0:T(128)S(1)} %add_rsqrt_fusion.1, bf16[1,2048]{1,0:T(2,128)(2,1)} %param.15, bf16[16,2048]{1,0:T(8,128)(2,1)S(1)} %copy-done.2), kind=kOutput, calls=%fused_computation.10 | convolution fusion | flops 18073856 | bytes 1135172 | tf_op jit(solution)/shard_map/dot_general | solution.py:45
  3.8 0.6 copy-done.6
  4.7 32.5 %all_gather.6 = bf16[128,2,128]{2,1,0:T(2,128)(2,1)S(1)} all-gather(bf16[16,2,128]{2,1,0:T(2,128)(2,1)S(1)} %slice.73), channel_id=1, replica_groups=mesh['kv'=8,'tp'=4] {'kv'}, dimensions={0}, use_global_device_ids=true | all-gather | bytes 73728 | tf_op jit(solution)/shard_map/all_gather | solution.py:95
  38.6 0.6 constant_dynamic-update-slice_fusion.7
  40.5 0.6 constant_dynamic-update-slice_fusion.4
  41.7 0.6 constant_dynamic-update-slice_fusion.2
  43.0 5.5 %all-to-all-start.2 = ((f32[8,2,16]{2,1,0:T(2,128)}), f32[8,2,16]{2,1,0:T(2,128)S(1)}, u32[]{:S(2)}, u32[]{:S(2)}) async-start(f32[8,2,16]{2,1,0:T(2,128)} %constant_dynamic-update-slice_fusion.1), calls=%async_computation.2 | async-start | bytes 16384 | tf_op jit(solution)/shard_map/all_to_all | solution.py:130
  48.8 1.9 %slice_bitcast_fusion = (bf16[2048,2,64]{2,1,0:T(2,128)(2,1)S(1)}, bf16[2048,2,64]{2,1,0:T(2,128)(2,1)S(1)}) fusion(bf16[1,2048,2,128]{3,2,1,0:T(2,128)(2,1)S(1)} %copy-done.1), kind=kLoop, calls=%fused_computation.16 | loop fusion | bytes 2097152 | tf_op jit(solution)/shard_map/reshape.43
  53.4 0.7 copy-done.7
  55.2 0.6 copy-done.10
  56.6 6.1 %all-to-all-start = ((f32[2,8,16]{2,0,1:T(2,128)}), f32[2,8,16]{2,0,1:T(2,128)S(1)}, u32[]{:S(2)}, u32[]{:S(2)}) async-start(f32[2,8,16]{2,0,1:T(2,128)} %copy.74), calls=%async_computation | async-start | bytes 16384 | tf_op jit(solution)/shard_map/all_to_all | solution.py:128
  63.4 5.8 %all-to-all-done = f32[2,8,16]{2,0,1:T(2,128)S(1)} async-done(((f32[2,8,16]{2,0,1:T(2,128)}), f32[2,8,16]{2,0,1:T(2,128)S(1)}, u32[]{:S(2)}, u32[]{:S(2)}) %all-to-all-start) | async-done | bytes 1056 | tf_op jit(solution)/shard_map/all_to_all | solution.py:128
  69.2 3.3 %all-to-all-start.3 = ((f32[2,8,16]{2,0,1:T(2,128)}), f32[2,8,16]{2,0,1:T(2,128)S(1)}, u32[]{:S(2)}, u32[]{:S(2)}) async-start(f32[2,8,16]{2,0,1:T(2,128)} %copy.82), calls=%async_computation.3 | async-start | bytes 16384 | tf_op jit(solution)/shard_map/all_to_all | solution.py:135
  72.8 0.7 convert_element_type.95
  74.3 0.7 convert_element_type.100
  74.9 4.1 %all-to-all-done.3 = f32[2,8,16]{2,0,1:T(2,128)S(1)} async-done(((f32[2,8,16]{2,0,1:T(2,128)}), f32[2,8,16]{2,0,1:T(2,128)S(1)}, u32[]{:S(2)}, u32[]{:S(2)}) %all-to-all-start.3) | async-done | bytes 1056 | tf_op jit(solution)/shard_map/all_to_all | solution.py:135
  79.0 3.3 %all-to-all-start.5 = ((f32[2,8,16]{2,0,1:T(2,128)}), f32[2,8,16]{2,0,1:T(2,128)S(1)}, u32[]{:S(2)}, u32[]{:S(2)}) async-start(f32[2,8,16]{2,0,1:T(2,128)} %copy.85), calls=%async_computation.5 | async-start | bytes 16384 | tf_op jit(solution)/shard_map/all_to_all | solution.py:136
  82.8 6.0 %all-to-all-done.5 = f32[2,8,16]{2,0,1:T(2,128)S(1)} async-done(((f32[2,8,16]{2,0,1:T(2,128)}), f32[2,8,16]{2,0,1:T(2,128)S(1)}, u32[]{:S(2)}, u32[]{:S(2)}) %all-to-all-start.5) | async-done | bytes 1056 | tf_op jit(solution)/shard_map/all_to_all | solution.py:136
  88.8 3.3 %all-to-all-start.1 = ((bf16[8,16,256]{2,1,0:T(8,128)(2,1)}), bf16[8,16,256]{2,1,0:T(8,128)(2,1)S(1)}, u32[]{:S(2)}, u32[]{:S(2)}) async-start(bf16[8,16,256]{2,1,0:T(8,128)(2,1)} %convert_element_type.95), calls=%async_computation.1 | async-start | bytes 131072 | tf_op jit(solution)/shard_map/all_to_all | solution.py:120
  92.8 6.2 %all-to-all-done.1 = bf16[8,16,256]{2,1,0:T(8,128)(2,1)S(1)} async-done(((bf16[8,16,256]{2,1,0:T(8,128)(2,1)}), bf16[8,16,256]{2,1,0:T(8,128)(2,1)S(1)}, u32[]{:S(2)}, u32[]{:S(2)}) %all-to-all-start.1) | async-done | bytes 65568 | tf_op jit(solution)/shard_map/all_to_all | solution.py:120
  99.0 3.3 %all-to-all-start.4 = ((bf16[8,16,256]{2,1,0:T(8,128)(2,1)}), bf16[8,16,256]{2,1,0:T(8,128)(2,1)S(1)}, u32[]{:S(2)}, u32[]{:S(2)}) async-start(bf16[8,16,256]{2,1,0:T(8,128)(2,1)} %convert_element_type.100), calls=%async_computation.4 | async-start | bytes 131072 | tf_op jit(solution)/shard_map/all_to_all | solution.py:123
  102.4 6.8 %all-to-all-done.4 = bf16[8,16,256]{2,1,0:T(8,128)(2,1)S(1)} async-done(((bf16[8,16,256]{2,1,0:T(8,128)(2,1)}), bf16[8,16,256]{2,1,0:T(8,128)(2,1)S(1)}, u32[]{:S(2)}, u32[]{:S(2)}) %all-to-all-start.4) | async-done | bytes 65568 | tf_op jit(solution)/shard_map/all_to_all | solution.py:123
  109.8 5.2 %all_gather.7 = bf16[17,1024]{1,0:T(8,128)(2,1)S(1)} all-gather(bf16[17,256]{1,0:T(8,128)(2,1)S(1)} %fusion.30), channel_id=1, replica_groups=mesh['kv'=8,'tp'=4] {'tp'}, dimensions={1}, use_global_device_ids=true | all-gather | bytes 43520 | tf_op jit(solution)/shard_map/all_gather | solution.py:203
  (101 shorter events, 13.4 us)
Async XLA Ops:
  0.6 52.3 %copy-start = (bf16[1,2048,2,128]{3,2,1,0:T(2,128)(2,1)S(1)}, bf16[1,2048,2,128]{3,2,1,0:T(2,128)(2,1)}, u32[]{:S(2)}) copy-start(bf16[1,2048,2,128]{3,2,1,0:T(2,128)(2,1)} %param.26) | copy-start | bytes 3145732
  0.6 1.2 %copy-start.2 = (bf16[16,2048]{1,0:T(8,128)(2,1)S(1)}, bf16[16,2048]{1,0:T(8,128)(2,1)}, u32[]{:S(2)}) copy-start(bf16[16,2048]{1,0:T(8,128)(2,1)} %param.14) | copy-start | bytes 196612
  0.7 2.8 %copy-start.3 = (bf16[2048,256]{1,0:T(8,128)(2,1)S(1)}, bf16[2048,256]{1,0:T(8,128)(2,1)}, u32[]{:S(2)}) copy-start(bf16[2048,256]{1,0:T(8,128)(2,1)} %param.17) | copy-start | bytes 3145732
  1.8 1.6 %copy-start.8 = (bf16[1,2048]{1,0:T(2,128)(2,1)S(1)}, bf16[1,2048]{1,0:T(2,128)(2,1)}, u32[]{:S(2)}) copy-start(bf16[1,2048]{1,0:T(2,128)(2,1)} %param.15) | copy-start | bytes 12292
  1.8 1.6 %copy-start.9 = (f32[2048]{0:T(1024)S(1)}, f32[2048]{0:T(1024)}, u32[]{:S(2)}) copy-start(f32[2048]{0:T(1024)} %param.16) | copy-start | bytes 24580
  3.5 1.0 copy-start.6
  4.7 44.1 %copy-start.1 = (bf16[1,2048,2,128]{3,2,1,0:T(2,128)(2,1)S(1)}, bf16[1,2048,2,128]{3,2,1,0:T(2,128)(2,1)}, u32[]{:S(2)}) copy-start(bf16[1,2048,2,128]{3,2,1,0:T(2,128)(2,1)} %param.25) | copy-start | bytes 3145732
  43.0 13.6 %all-to-all-start.2 = ((f32[8,2,16]{2,1,0:T(2,128)}), f32[8,2,16]{2,1,0:T(2,128)S(1)}, u32[]{:S(2)}, u32[]{:S(2)}) async-start(f32[8,2,16]{2,1,0:T(2,128)} %constant_dynamic-update-slice_fusion.1), calls=%async_computation.2 | async-start | bytes 16384 | tf_op jit(solution)/shard_map/all_to_all | solution.py:130
  48.8 2.6 %copy-start.4 = (bf16[2048,256]{1,0:T(8,128)(2,1)S(1)}, bf16[2048,256]{1,0:T(8,128)(2,1)}, u32[]{:S(2)}) copy-start(bf16[2048,256]{1,0:T(8,128)(2,1)} %param.19) | copy-start | bytes 3145732
  53.2 1.0 copy-start.7
  55.1 0.7 copy-start.10
  56.6 6.1 %copy-start.11 = (f32[128]{0:T(128)S(1)}, f32[128]{0:T(128)}, u32[]{:S(2)}) copy-start(f32[128]{0:T(128)} %param.21) | copy-start | bytes 1540
  56.6 12.7 %all-to-all-start = ((f32[2,8,16]{2,0,1:T(2,128)}), f32[2,8,16]{2,0,1:T(2,128)S(1)}, u32[]{:S(2)}, u32[]{:S(2)}) async-start(f32[2,8,16]{2,0,1:T(2,128)} %copy.74), calls=%async_computation | async-start | bytes 16384 | tf_op jit(solution)/shard_map/all_to_all | solution.py:128
  69.2 9.8 %all-to-all-start.3 = ((f32[2,8,16]{2,0,1:T(2,128)}), f32[2,8,16]{2,0,1:T(2,128)S(1)}, u32[]{:S(2)}, u32[]{:S(2)}) async-start(f32[2,8,16]{2,0,1:T(2,128)} %copy.82), calls=%async_computation.3 | async-start | bytes 16384 | tf_op jit(solution)/shard_map/all_to_all | solution.py:135
  79.0 9.8 %all-to-all-start.5 = ((f32[2,8,16]{2,0,1:T(2,128)}), f32[2,8,16]{2,0,1:T(2,128)S(1)}, u32[]{:S(2)}, u32[]{:S(2)}) async-start(f32[2,8,16]{2,0,1:T(2,128)} %copy.85), calls=%async_computation.5 | async-start | bytes 16384 | tf_op jit(solution)/shard_map/all_to_all | solution.py:136
  82.7 32.3 %copy-start.5 = (bf16[1024,512]{1,0:T(8,128)(2,1)S(1)}, bf16[1024,512]{1,0:T(8,128)(2,1)}, u32[]{:S(2)}) copy-start(bf16[1024,512]{1,0:T(8,128)(2,1)} %param.20) | copy-start | bytes 3145732
  88.8 10.2 %all-to-all-start.1 = ((bf16[8,16,256]{2,1,0:T(8,128)(2,1)}), bf16[8,16,256]{2,1,0:T(8,128)(2,1)S(1)}, u32[]{:S(2)}, u32[]{:S(2)}) async-start(bf16[8,16,256]{2,1,0:T(8,128)(2,1)} %convert_element_type.95), calls=%async_computation.1 | async-start | bytes 131072 | tf_op jit(solution)/shard_map/all_to_all | solution.py:120
  99.0 10.2 %all-to-all-start.4 = ((bf16[8,16,256]{2,1,0:T(8,128)(2,1)}), bf16[8,16,256]{2,1,0:T(8,128)(2,1)S(1)}, u32[]{:S(2)}, u32[]{:S(2)}) async-start(bf16[8,16,256]{2,1,0:T(8,128)(2,1)} %convert_element_type.100), calls=%async_computation.4 | async-start | bytes 131072 | tf_op jit(solution)/shard_map/all_to_all | solution.py:123
